TPU v7x, 256 devices: a whole 4x4x8 slice. The times are simulated.
256 devices in a mesh: fs: 32 (over z, x), tp: 8 (over y, core).
Axes of the slice: x: 4, y: 4, z: 8, core: 2. Of those that a mesh axis runs over, the one named last changes fastest.
Arguments:
- later_rows: bfloat16 [32768, 2048], P(('fs', 'tp')), may hold values from -6 to 6
- earlier_rows: bfloat16 [32768, 2048], P(('fs', 'tp')), may hold values from -6 to 6
- cotangent: bfloat16 [32768, 2048], P(('fs', 'tp')), may hold values from -24 to 24
- up_weight: bfloat16 [2048, 4096], P('fs', 'tp'), may hold values from -0.125 to 0.125
- down_weight: bfloat16 [2048, 4096], P('fs', 'tp'), may hold values from -0.09375 to 0.09375
- up_total: float32 [2048, 4096], P('fs', 'tp'), may hold values from -6 to 6
- down_total: float32 [2048, 4096], P('fs', 'tp'), may hold values from -6 to 6
Outputs:
- later_out: bfloat16 [32768, 2048], P(('fs', 'tp'))
- earlier_grad: bfloat16 [32768, 2048], P(('fs', 'tp'))
- up_updated: float32 [2048, 4096], P('fs', 'tp')
- down_updated: float32 [2048, 4096], P('fs', 'tp')
All inputs are finite; a program needn't handle non-finite values.
Results may differ from a plain program's by a relative error of at most 0.015.
Values may be sent and summed in bfloat16 or wider, within the bound.
No kernel may reach another device: no remote copies, remote signals or barrier semaphores. Data moves between devices by JAX's collectives and lax.ppermute only.
A program may use at most 128 MiB of HBM per device.

v0:
```python
import math
import jax
import jax.numpy as jnp
from jax import lax
from jax.sharding import Mesh
from jax.sharding import PartitionSpec as P

FS = ("fs_0", "fs_1")
FS_TP = ("fs_0", "fs_1", "tp")


def side_by_side(arrays, axis, dim, along):
    ends, at = ([], 0)
    for a in arrays[:-1]:
        at += a.shape[along]
        ends.append(at)
    both = jnp.concatenate(arrays, axis=along)
    return tuple(jnp.split(lax.all_gather(both, axis, axis=dim, tiled=True), ends, axis=along))


def in_blocks(x, dim, length):
    before, after = (x.shape[:dim], x.shape[dim + 1 :])
    return jnp.moveaxis(x.reshape(*before, length, -1, *after), dim, 0)


def sum_at_owner(x, axis, dim):
    length = lax.axis_size(axis)
    tiles = lax.all_to_all(in_blocks(x, dim, length), axis, 0, 0, tiled=True)
    return jnp.sum(tiles.astype(jnp.float32), axis=0)


def sum_by_axis(terms, axes):
    subtotal = terms.astype(jnp.bfloat16)
    for axis in axes:
        subtotal = lax.psum_scatter(subtotal, axis, scatter_dimension=0, tiled=True)
    return subtotal.astype(jnp.float32)


def contract_last(left, right):
    return lax.dot_general(
        left, right, (((1,), (1,)), ((), ())), preferred_element_type=jnp.float32
    )


def body(later_rows, earlier_rows, cotangent, up_weight, down_weight, up_total, down_total):
    rows_dev = later_rows.shape[0]
    total_rows = rows_dev * lax.axis_size(FS) * lax.axis_size("tp")
    factor = 1.0 / math.sqrt(total_rows)
    up_full, down_full = side_by_side((up_weight, down_weight), FS, 0, 1)

    def fetch():
        return (up_full, down_full)

    def to_owner(term):
        return sum_at_owner(term.astype(jnp.bfloat16), "tp", 0)

    def grad_owner(group, right):
        return sum_by_axis(
            lax.dot_general(
                group, right, (((0,), (0,)), ((), ())), preferred_element_type=jnp.float32
            ),
            FS,
        )

    up_whole, down_whole = fetch()
    group = lax.all_gather(later_rows, "tp", axis=0, tiled=True)
    relu_part = jnp.maximum(jnp.dot(group, up_whole, preferred_element_type=jnp.float32), 0.0)
    hidden = (relu_part * relu_part).astype(jnp.bfloat16)
    partial_value = contract_last(hidden, down_whole)
    later_out = to_owner(partial_value).astype(jnp.bfloat16)
    up_whole, down_whole = fetch()
    saved_group, cot_group = side_by_side((earlier_rows, cotangent), "tp", 0, 1)
    relu_part = jnp.maximum(jnp.dot(saved_group, up_whole, preferred_element_type=jnp.float32), 0.0)
    hidden = (relu_part * relu_part).astype(jnp.bfloat16)
    hidden_grad = jnp.dot(cot_group, down_whole, preferred_element_type=jnp.float32)
    pre_grad = (2.0 * relu_part * hidden_grad).astype(jnp.bfloat16)
    input_partial = contract_last(pre_grad, up_whole)
    earlier_grad = to_owner(input_partial).astype(jnp.bfloat16)
    down_updated = down_total + grad_owner(cot_group, hidden) * factor
    up_updated = up_total + grad_owner(saved_group, pre_grad) * factor
    earlier_grad, up_updated, down_updated = (earlier_grad, up_updated, down_updated)
    return (later_out, earlier_grad, up_updated, down_updated)


def solution(mesh):
    finer = Mesh(mesh.devices.reshape(8, 4, mesh.shape["tp"]), ("fs_0", "fs_1", "tp"))
    placed = (
        P(FS_TP, None),
        P(FS_TP, None),
        P(FS_TP, None),
        P(FS, "tp"),
        P(FS, "tp"),
        P(FS, "tp"),
        P(FS, "tp"),
    )
    return jax.shard_map(
        body,
        mesh=finer,
        in_specs=placed,
        out_specs=(P(FS_TP, None), P(FS_TP, None), P(FS, "tp"), P(FS, "tp")),
        check_vma=False,
    )
```

profile of v0, /device:TPU:8, one launch (start us, length us, event | category | flops | bytes accessed | tf_op | source)
XLA Modules:
  0.0 330.6 jit_solution(11753121503092980763)
XLA Ops:
  7.2 0.0 all-gather.4.cloned.1.call-start
  7.2 1.5 pad_maximum_fusion.1
  8.7 0.0 all-gather.4.cloned.1.call-update
  8.8 0.0 all-gather.8.cloned.1.call-start
  8.8 2.3 pad_maximum_fusion
  11.1 0.0 all-gather.8.cloned.1.call-update
  11.1 0.0 all-gather.6.cloned.1.call-start
  11.2 0.7 all-gather.6.cloned.1.call-update
  11.9 0.0 reduce-scatter.9.cloned.1.call-start
  11.9 83.9 %all-gather.4.cloned.1.call-done = bf16[2048,1024]{1,0:T(8,128)(2,1)} async-done(((bf16[64,1024]{1,0:T(8,128)(2,1)}), bf16[2048,1024]{1,0:T(8,128)(2,1)}) %all-gather.4.cloned.1.call-update) | async-done | bytes 4194320 | tf_op jit(solution)/shard_map/all_gather | solution.py:18
  95.8 50.1 %all-gather.8.cloned.1.call-done = bf16[1024,4096]{1,0:T(8,128)(2,1)} async-done(((bf16[128,4096]{1,0:T(8,128)(2,1)}), bf16[1024,4096]{1,0:T(8,128)(2,1)}) %all-gather.8.cloned.1.call-update) | async-done | bytes 8388624 | tf_op jit(solution)/shard_map/all_gather | solution.py:18
  145.9 5.3 %fusion.6 = f32[1024,512]{1,0:T(8,128)S(1)} fusion(bf16[1024,4096]{1,0:T(8,128)(2,1)} %all-gather.8.cloned.1.call-done, bf16[2048,1024]{1,0:T(8,128)(2,1)} %all-gather.4.cloned.1.call-done), kind=kOutput, calls=%fused_computation.8 | convolution fusion | flops 2147483648 | bytes 8388608 | tf_op jit(solution)/shard_map/dot_general | solution.py:73
  151.2 3.7 %fusion.11 = bf16[2048,512]{1,0:T(8,128)(2,1)} fusion(bf16[1024,4096]{1,0:T(8,128)(2,1)S(1)} %copy-done.2, f32[1024,512]{1,0:T(8,128)S(1)} %fusion.6), kind=kOutput, calls=%fused_computation.11 | convolution fusion | flops 2150105088 | bytes 8388608 | tf_op jit(solution)/shard_map/dot_general | solution.py:59
  155.0 27.4 %all-gather.6.cloned.1.call-done = bf16[1024,2048]{1,0:T(8,128)(2,1)} async-done(((bf16[128,2048]{1,0:T(8,128)(2,1)}), bf16[1024,2048]{1,0:T(8,128)(2,1)}) %all-gather.6.cloned.1.call-update) | async-done | bytes 4194320 | tf_op jit(solution)/shard_map/all_gather | solution.py:66
  182.4 10.0 %convolution_convert_fusion.1 = bf16[1024,2048]{1,0:T(8,128)(2,1)} fusion(bf16[2048,1024]{1,0:T(8,128)(2,1)} %all-gather.4.cloned.1.call-done, bf16[1024,2048]{1,0:T(8,128)(2,1)} %all-gather.6.cloned.1.call-done), kind=kOutput, calls=%fused_computation.1 | convolution fusion | flops 4298637312 | bytes 12582912 | tf_op jit(solution)/shard_map/dot_general | solution.py:40
  192.4 6.0 %all-to-all-start = ((bf16[8,128,2048]{2,1,0:T(8,128)(2,1)}), bf16[8,128,2048]{2,1,0:T(8,128)(2,1)}, u32[]{:S(2)}, u32[]{:S(2)}) async-start(bf16[8,128,2048]{2,1,0:T(8,128)(2,1)} %bitcast.6), calls=%async_computation | async-start | bytes 8388608 | tf_op jit(solution)/shard_map/all_to_all | solution.py:28
  198.4 5.2 %multiply_convert_fusion.1 = bf16[1024,512]{1,0:T(8,128)(2,1)S(1)} fusion(f32[1024,512]{1,0:T(8,128)S(1)} %fusion.6, bf16[2048,1024]{1,0:T(8,128)(2,1)} %all-gather.4.cloned.1.call-done, bf16[1024,4096]{1,0:T(8,128)(2,1)} %all-gather.8.cloned.1.call-done), kind=kOutput, calls=%fused_computation.13 | convolution fusion | flops 2149580800 | bytes 9437184 | tf_op jit(solution)/shard_map/dot_general | solution.py:75
  203.6 6.0 %fusion.8 = bf16[2048,512]{1,0:T(8,128)(2,1)} fusion(bf16[1024,512]{1,0:T(8,128)(2,1)S(1)} %multiply_convert_fusion.1, bf16[1024,4096]{1,0:T(8,128)(2,1)} %all-gather.8.cloned.1.call-done), kind=kOutput, calls=%fused_computation.10 | convolution fusion | flops 2148532224 | bytes 7340032 | tf_op jit(solution)/shard_map/dot_general | solution.py:59
  209.5 0.0 reduce-scatter.5.cloned.1.call-update
  209.6 5.9 %convolution_convert_fusion = bf16[1024,2048]{1,0:T(8,128)(2,1)} fusion(bf16[1024,512]{1,0:T(8,128)(2,1)S(1)} %multiply_convert_fusion.1, bf16[2048,1024]{1,0:T(8,128)(2,1)} %all-gather.4.cloned.1.call-done), kind=kOutput, calls=%fused_computation | convolution fusion | flops 2149580800 | bytes 7340032 | tf_op jit(solution)/shard_map/dot_general | solution.py:40
  215.5 31.2 %all-to-all-done = bf16[8,128,2048]{2,1,0:T(8,128)(2,1)} async-done(((bf16[8,128,2048]{2,1,0:T(8,128)(2,1)}), bf16[8,128,2048]{2,1,0:T(8,128)(2,1)}, u32[]{:S(2)}, u32[]{:S(2)}) %all-to-all-start) | async-done | bytes 4194336 | tf_op jit(solution)/shard_map/all_to_all | solution.py:28
  246.7 5.9 %all-to-all-start.1 = ((bf16[8,128,2048]{2,1,0:T(8,128)(2,1)}), bf16[8,128,2048]{2,1,0:T(8,128)(2,1)}, u32[]{:S(2)}, u32[]{:S(2)}) async-start(bf16[8,128,2048]{2,1,0:T(8,128)(2,1)} %bitcast.5), calls=%async_computation.1 | async-start | bytes 8388608 | tf_op jit(solution)/shard_map/all_to_all | solution.py:28
  252.6 0.6 reduce-scatter.11.cloned.1.call-update
  253.2 0.0 reduce-scatter.7.cloned.1.call-start
  253.2 18.8 %reduce-scatter.5.cloned.1.call-done = bf16[256,512]{1,0:T(8,128)(2,1)} async-done(((bf16[2048,512]{1,0:T(8,128)(2,1)}), bf16[256,512]{1,0:T(8,128)(2,1)}) %reduce-scatter.5.cloned.1.call-update) | async-done | bytes 262160 | tf_op jit(solution)/shard_map/reduce_scatter | solution.py:35
  272.0 0.0 reduce-scatter.7.cloned.1.call-update
  272.0 3.9 %reduce_sum.24 = bf16[128,2048]{1,0:T(8,128)(2,1)} reduce(bf16[8,128,2048]{2,1,0:T(8,128)(2,1)} %all-to-all-done, bf16[]{:T(256)} %constant.3.clone.1), dimensions={0}, to_apply=%region_0.0 | reduce | flops 1835008 | bytes 4718594 | tf_op jit(solution)/shard_map/reduce_sum | solution.py:29
  275.9 25.0 %all-to-all-done.1 = bf16[8,128,2048]{2,1,0:T(8,128)(2,1)} async-done(((bf16[8,128,2048]{2,1,0:T(8,128)(2,1)}), bf16[8,128,2048]{2,1,0:T(8,128)(2,1)}, u32[]{:S(2)}, u32[]{:S(2)}) %all-to-all-start.1) | async-done | bytes 4194336 | tf_op jit(solution)/shard_map/all_to_all | solution.py:28
  300.9 3.8 %reduce_sum.25 = bf16[128,2048]{1,0:T(8,128)(2,1)} reduce(bf16[8,128,2048]{2,1,0:T(8,128)(2,1)} %all-to-all-done.1, bf16[]{:T(256)} %constant.3.clone.1), dimensions={0}, to_apply=%region_1.0 | reduce | flops 1835008 | bytes 4718594 | tf_op jit(solution)/shard_map/reduce_sum | solution.py:29
  304.8 1.5 multiply_add_fusion
  306.3 16.0 %reduce-scatter.7.cloned.1.call-done = bf16[64,512]{1,0:T(8,128)(2,1)} async-done(((bf16[256,512]{1,0:T(8,128)(2,1)}), bf16[64,512]{1,0:T(8,128)(2,1)}) %reduce-scatter.7.cloned.1.call-update) | async-done | bytes 65552 | tf_op jit(solution)/shard_map/reduce_scatter | solution.py:35
  322.3 1.5 multiply_add_fusion.1
  (11 shorter events, 0.0 us)
Async XLA Ops:
  7.2 88.6 %all-gather.4.cloned.1.call-start = ((), (), s32[]{:S(2)}) async-start(), calls=%async_computation.6 | async-start | bytes 4325376 | tf_op jit(solution)/shard_map/all_gather | solution.py:18
  8.8 137.1 %all-gather.8.cloned.1.call-start = ((), (), s32[]{:S(2)}) async-start(), calls=%async_computation.8 | async-start | bytes 9437184 | tf_op jit(solution)/shard_map/all_gather | solution.py:18
  11.1 171.2 %all-gather.6.cloned.1.call-start = ((), (), s32[]{:S(2)}) async-start(), calls=%async_computation.7 | async-start | bytes 4718592 | tf_op jit(solution)/shard_map/all_gather | solution.py:66
  11.9 240.7 %reduce-scatter.9.cloned.1.call-start = ((), (), s32[]{:S(2)}) async-start(), calls=%async_computation.11 | async-start | bytes 2359296 | tf_op jit(solution)/shard_map/reduce_scatter | solution.py:35
  145.9 5.3 %copy-start.2 = (bf16[1024,4096]{1,0:T(8,128)(2,1)S(1)}, bf16[1024,4096]{1,0:T(8,128)(2,1)}, u32[]{:S(2)}) copy-start(bf16[1024,4096]{1,0:T(8,128)(2,1)} %all-gather.8.cloned.1.call-done) | copy-start | bytes 25165828
  192.4 54.3 %all-to-all-start = ((bf16[8,128,2048]{2,1,0:T(8,128)(2,1)}), bf16[8,128,2048]{2,1,0:T(8,128)(2,1)}, u32[]{:S(2)}, u32[]{:S(2)}) async-start(bf16[8,128,2048]{2,1,0:T(8,128)(2,1)} %bitcast.6), calls=%async_computation | async-start | bytes 8388608 | tf_op jit(solution)/shard_map/all_to_all | solution.py:28
  198.4 73.6 %reduce-scatter.5.cloned.1.call-start = ((), (), s32[]{:S(2)}) async-start(), calls=%async_computation.9 | async-start | bytes 2359296 | tf_op jit(solution)/shard_map/reduce_scatter | solution.py:35
  246.7 54.2 %all-to-all-start.1 = ((bf16[8,128,2048]{2,1,0:T(8,128)(2,1)}), bf16[8,128,2048]{2,1,0:T(8,128)(2,1)}, u32[]{:S(2)}, u32[]{:S(2)}) async-start(bf16[8,128,2048]{2,1,0:T(8,128)(2,1)} %bitcast.5), calls=%async_computation.1 | async-start | bytes 8388608 | tf_op jit(solution)/shard_map/all_to_all | solution.py:28
  252.6 52.2 %reduce-scatter.11.cloned.1.call-start = ((), (), s32[]{:S(2)}) async-start(), calls=%async_computation.12 | async-start | bytes 327680 | tf_op jit(solution)/shard_map/reduce_scatter | solution.py:35
  253.2 69.1 %reduce-scatter.7.cloned.1.call-start = ((), (), s32[]{:S(2)}) async-start(), calls=%async_computation.10 | async-start | bytes 327680 | tf_op jit(solution)/shard_map/reduce_scatter | solution.py:35
  272.0 32.8 %copy-start = (f32[64,512]{1,0:T(8,128)S(1)}, f32[64,512]{1,0:T(8,128)}, u32[]{:S(2)}) copy-start(f32[64,512]{1,0:T(8,128)} %param.13) | copy-start | bytes 393220
  272.0 50.3 %copy-start.1 = (f32[64,512]{1,0:T(8,128)S(1)}, f32[64,512]{1,0:T(8,128)}, u32[]{:S(2)}) copy-start(f32[64,512]{1,0:T(8,128)} %param.12) | copy-start | bytes 393220
Sparse Core Ops, SparseCore 0:
  11.1 84.6 all-gather.3
  97.6 48.1 all-gather.7
  147.8 34.5 all-gather.5
  184.8 43.4 reduce-scatter.8
  230.7 41.2 reduce-scatter.4
  274.3 22.1 reduce-scatter.10
  299.1 23.1 reduce-scatter.6
where the time goes:
time: 331 us
  waiting for transfers between devices  254 us (77%)
  matrix products  36.1 us (11%)
  other arithmetic  14.6 us (4%)
  between operations  14.2 us (4%)
  starting transfers between devices  12.1 us (4%)
    all_gather x2, waiting for transfers between devices, side_by_side(): lax.all_gather(both, axis, axis=dim, tiled=True)  134 us
    all_to_all x2, waiting for transfers between devices, sum_at_owner(): tiles = lax.all_to_all(in_blocks(x, dim, length), axis, 0, 0, tiled=True)  56.2 us
    reduce_scatter x4, waiting for transfers between devices, sum_by_axis(): subtotal = lax.psum_scatter(subtotal, axis, scatter_dimension=0, tiled=True)  34.8 us
    all_gather x1, waiting for transfers between devices, body(): group = lax.all_gather(later_rows, 'tp', axis=0, tiled=True)  27.4 us
    dot_general x2, matrix products, contract_last(): lax.dot_general(left, right, (((1,), (1,)), ((), ())), preferred_element_...  15.9 us
    all_to_all x2, starting transfers between devices, sum_at_owner(): tiles = lax.all_to_all(in_blocks(x, dim, length), axis, 0, 0, tiled=True)  11.9 us
    dot_general x2, matrix products, grad_owner(): lax.dot_general(group, right, (((0,), (0,)), ((), ())), preferred_element...  9.68 us
    reduce_sum x2, other arithmetic, sum_at_owner(): return jnp.sum(tiles.astype(jnp.float32), axis=0)  7.73 us
  transfers between devices with their start and end apart: 9, of which 7 were waited for; matrix products, arithmetic and copies ran while one was open for 14% of the time, Pallas kernels for 0%

commit v1 on v0

--- a/solution.py
+++ b/solution.py
@@ -7,6 +7,29 @@
 
 FS = ("fs_0", "fs_1")
 FS_TP = ("fs_0", "fs_1", "tp")
+
+
+def laid_out(blocks, dim):
+    lengths = list(blocks.shape[1:])
+    lengths[dim] *= blocks.shape[0]
+    return jnp.moveaxis(blocks, 0, dim).reshape(lengths)
+
+
+def grow_blocks(array, axis):
+    count, index = (lax.axis_size(axis), lax.axis_index(axis))
+    blocks, distance = (array[None], 1)
+    while distance < count:
+        partner_block = lax.ppermute(blocks, axis, [(i, i ^ distance) for i in range(count)])
+        low = index & distance == 0
+        blocks = jnp.concatenate(
+            [jnp.where(low, blocks, partner_block), jnp.where(low, partner_block, blocks)]
+        )
+        distance *= 2
+    return blocks
+
+
+def collect(x, axis, dim):
+    return laid_out(grow_blocks(x, axis), dim)
 
 
 def side_by_side(arrays, axis, dim, along):
@@ -63,7 +86,7 @@
         )
 
     up_whole, down_whole = fetch()
-    group = lax.all_gather(later_rows, "tp", axis=0, tiled=True)
+    group = collect(later_rows, "tp", 0)
     relu_part = jnp.maximum(jnp.dot(group, up_whole, preferred_element_type=jnp.float32), 0.0)
     hidden = (relu_part * relu_part).astype(jnp.bfloat16)
     partial_value = contract_last(hidden, down_whole)

time: 331 us -> 303 us (0.915)
  waiting for transfers between devices: 254 us -> 212 us
  other arithmetic: 14.6 us -> 21.8 us
  starting transfers between devices: 12.1 us -> 16.2 us
    all_gather x2, waiting for transfers between devices: 134 us -> 102 us  [side_by_side(): lax.all_gather(both, axis, axis=dim, tiled=True)]
    all_gather x1 -> x0, waiting for transfers between devices: 27.4 us -> none  [body(): group = lax.all_gather(later_rows, 'tp', axis=0, tiled=True)]
    ppermute x0 -> x3, waiting for transfers between devices: none -> 25.5 us  [grow_blocks(): lax.ppermute(blocks, axis, [(i, i ^ distance) for i in range(count)])]
    reduce_scatter x4, waiting for transfers between devices: 34.8 us -> 21.8 us  [sum_by_axis(): subtotal = lax.psum_scatter(subtotal, axis, scatter_dimension=0, tiled=True)]
    all_to_all x2, waiting for transfers between devices: 56.2 us -> 62.4 us  [sum_at_owner(): tiles = lax.all_to_all(in_blocks(x, dim, length), axis, 0, 0, tiled=True)]
    ppermute x0 -> x3, starting transfers between devices: none -> 4.21 us  [grow_blocks(): lax.ppermute(blocks, axis, [(i, i ^ distance) for i in range(count)])]
    concatenate x0 -> x3, other arithmetic: none -> 3.94 us  [grow_blocks(): jnp.concatenate([jnp.where(low, blocks, partner_block), jnp.where(low, pa...]
  transfers between devices with their start and end apart: 9 -> 11, of which waited for: 7 -> 8; matrix products, arithmetic and copies ran while one was open for 14% -> 18% of each run, Pallas kernels for 0% -> 0%
where the time goes in v1:
time: 303 us; the launch traced here: 302 us
  waiting for transfers between devices  212 us (70%)
  matrix products  36.2 us (12%)
  other arithmetic  21.8 us (7%)
  starting transfers between devices  16.2 us (5%)
  between operations  14.2 us (5%)
    all_gather x2, waiting for transfers between devices, side_by_side(): lax.all_gather(both, axis, axis=dim, tiled=True)  102 us
    all_to_all x2, waiting for transfers between devices, sum_at_owner(): tiles = lax.all_to_all(in_blocks(x, dim, length), axis, 0, 0, tiled=True)  62.4 us
    ppermute x3, waiting for transfers between devices, grow_blocks(): lax.ppermute(blocks, axis, [(i, i ^ distance) for i in range(count)])  25.5 us
    reduce_scatter x4, waiting for transfers between devices, sum_by_axis(): subtotal = lax.psum_scatter(subtotal, axis, scatter_dimension=0, tiled=True)  21.8 us
    dot_general x2, matrix products, contract_last(): lax.dot_general(left, right, (((1,), (1,)), ((), ())), preferred_element_...  15.9 us
    all_to_all x2, starting transfers between devices, sum_at_owner(): tiles = lax.all_to_all(in_blocks(x, dim, length), axis, 0, 0, tiled=True)  11.8 us
    dot_general x2, matrix products, grad_owner(): lax.dot_general(group, right, (((0,), (0,)), ((), ())), preferred_element...  9.68 us
    reduce_sum x2, other arithmetic, sum_at_owner(): return jnp.sum(tiles.astype(jnp.float32), axis=0)  7.7 us
  transfers between devices with their start and end apart: 11, of which 8 were waited for; matrix products, arithmetic and copies ran while one was open for 18% of the time, Pallas kernels for 0%

profile of v1, /device:TPU:8, one launch (start us, length us, event | category | flops | bytes accessed | tf_op | source)
XLA Modules:
  0.0 302.1 jit_solution(2056050130769653822)
XLA Ops:
  7.2 1.6 pad_maximum_fusion.4
  8.9 2.3 pad_maximum_fusion.3
  11.3 0.1 collective-permute-start
  11.4 1.9 collective-permute-done
  13.3 0.1 pad_maximum_fusion.2
  13.4 2.2 collective-permute-start.1
  15.7 23.6 %collective-permute-done.1 = bf16[2,128,2048]{2,1,0:T(8,128)(2,1)} collective-permute-done((bf16[2,128,2048]{2,1,0:T(8,128)(2,1)S(1)}, bf16[2,128,2048]{2,1,0:T(8,128)(2,1)}, u32[]{:S(2)}, u32[]{:S(2)}) %collective-permute-start.1) | collective-permute-done | bytes 1048608 | tf_op jit(solution)/shard_map/ppermute | solution.py:22
  39.2 1.4 broadcast_select_fusion.3
  40.6 1.5 pad_maximum_fusion.1
  42.1 1.9 collective-permute-start.2
  44.0 51.8 %all-gather.3.cloned.1.call-done = bf16[2048,1024]{1,0:T(8,128)(2,1)} async-done(((bf16[64,1024]{1,0:T(8,128)(2,1)}), bf16[2048,1024]{1,0:T(8,128)(2,1)}) %all-gather.3.cloned.1.call-update) | async-done | bytes 4194320 | tf_op jit(solution)/shard_map/all_gather | solution.py:41
  95.8 50.1 %all-gather.5.cloned.1.call-done = bf16[1024,4096]{1,0:T(8,128)(2,1)} async-done(((bf16[128,4096]{1,0:T(8,128)(2,1)}), bf16[1024,4096]{1,0:T(8,128)(2,1)}) %all-gather.5.cloned.1.call-update) | async-done | bytes 8388624 | tf_op jit(solution)/shard_map/all_gather | solution.py:41
  145.9 5.3 %fusion.6 = f32[1024,512]{1,0:T(8,128)S(1)} fusion(bf16[1024,4096]{1,0:T(8,128)(2,1)} %all-gather.5.cloned.1.call-done, bf16[2048,1024]{1,0:T(8,128)(2,1)} %all-gather.3.cloned.1.call-done), kind=kOutput, calls=%fused_computation.9 | convolution fusion | flops 2147483648 | bytes 8388608 | tf_op jit(solution)/shard_map/dot_general | solution.py:96
  151.2 1.4 copy-done.4
  152.6 3.7 %fusion.11 = bf16[2048,512]{1,0:T(8,128)(2,1)} fusion(bf16[1024,4096]{1,0:T(8,128)(2,1)S(1)} %copy-done.3, f32[1024,512]{1,0:T(8,128)S(1)} %fusion.6), kind=kOutput, calls=%fused_computation.12 | convolution fusion | flops 2150105088 | bytes 8388608 | tf_op jit(solution)/shard_map/dot_general | solution.py:82
  156.3 1.9 broadcast_select_fusion.1
  158.2 2.3 pad_maximum_fusion
  160.6 9.9 %convolution_convert_fusion.1 = bf16[1024,2048]{1,0:T(8,128)(2,1)} fusion(bf16[2048,1024]{1,0:T(8,128)(2,1)} %all-gather.3.cloned.1.call-done, bf16[1024,2048]{1,0:T(8,128)(2,1)} %bitcast.11), kind=kOutput, calls=%fused_computation.2 | convolution fusion | flops 4298637312 | bytes 12582912 | tf_op jit(solution)/shard_map/dot_general | solution.py:63
  170.5 5.9 %all-to-all-start = ((bf16[8,128,2048]{2,1,0:T(8,128)(2,1)}), bf16[8,128,2048]{2,1,0:T(8,128)(2,1)}, u32[]{:S(2)}, u32[]{:S(2)}) async-start(bf16[8,128,2048]{2,1,0:T(8,128)(2,1)} %bitcast.10), calls=%async_computation | async-start | bytes 8388608 | tf_op jit(solution)/shard_map/all_to_all | solution.py:51
  176.4 5.2 %multiply_convert_fusion.1 = bf16[1024,512]{1,0:T(8,128)(2,1)S(1)} fusion(f32[1024,512]{1,0:T(8,128)S(1)} %copy-done.5, bf16[2048,1024]{1,0:T(8,128)(2,1)} %all-gather.3.cloned.1.call-done, bf16[1024,4096]{1,0:T(8,128)(2,1)} %all-gather.5.cloned.1.call-done), kind=kOutput, calls=%fused_computation.15 | convolution fusion | flops 2149580800 | bytes 9437184 | tf_op jit(solution)/shard_map/dot_general | solution.py:98
  181.7 6.0 %fusion.8 = bf16[2048,512]{1,0:T(8,128)(2,1)} fusion(bf16[1024,512]{1,0:T(8,128)(2,1)S(1)} %multiply_convert_fusion.1, bf16[1024,4096]{1,0:T(8,128)(2,1)} %all-gather.5.cloned.1.call-done), kind=kOutput, calls=%fused_computation.11 | convolution fusion | flops 2148532224 | bytes 7340032 | tf_op jit(solution)/shard_map/dot_general | solution.py:82
  187.7 6.0 %convolution_convert_fusion = bf16[1024,2048]{1,0:T(8,128)(2,1)} fusion(bf16[1024,512]{1,0:T(8,128)(2,1)S(1)} %multiply_convert_fusion.1, bf16[2048,1024]{1,0:T(8,128)(2,1)} %all-gather.3.cloned.1.call-done), kind=kOutput, calls=%fused_computation.1 | convolution fusion | flops 2149580800 | bytes 7340032 | tf_op jit(solution)/shard_map/dot_general | solution.py:63
  193.7 31.0 %all-to-all-done = bf16[8,128,2048]{2,1,0:T(8,128)(2,1)} async-done(((bf16[8,128,2048]{2,1,0:T(8,128)(2,1)}), bf16[8,128,2048]{2,1,0:T(8,128)(2,1)}, u32[]{:S(2)}, u32[]{:S(2)}) %all-to-all-start) | async-done | bytes 4194336 | tf_op jit(solution)/shard_map/all_to_all | solution.py:51
  224.8 5.9 %all-to-all-start.1 = ((bf16[8,128,2048]{2,1,0:T(8,128)(2,1)}), bf16[8,128,2048]{2,1,0:T(8,128)(2,1)}, u32[]{:S(2)}, u32[]{:S(2)}) async-start(bf16[8,128,2048]{2,1,0:T(8,128)(2,1)} %bitcast.9), calls=%async_computation.1 | async-start | bytes 8388608 | tf_op jit(solution)/shard_map/all_to_all | solution.py:51
  230.7 0.6 reduce-scatter.11.cloned.1.call-update
  231.3 12.4 %reduce-scatter.5.cloned.1.call-done = bf16[256,512]{1,0:T(8,128)(2,1)} async-done(((bf16[2048,512]{1,0:T(8,128)(2,1)}), bf16[256,512]{1,0:T(8,128)(2,1)}) %reduce-scatter.5.cloned.1.call-update) | async-done | bytes 262160 | tf_op jit(solution)/shard_map/reduce_scatter | solution.py:58
  243.7 3.8 %reduce_sum.24 = bf16[128,2048]{1,0:T(8,128)(2,1)} reduce(bf16[8,128,2048]{2,1,0:T(8,128)(2,1)} %all-to-all-done, bf16[]{:T(256)} %constant.8.clone.1), dimensions={0}, to_apply=%region_0.1 | reduce | flops 1835008 | bytes 4718594 | tf_op jit(solution)/shard_map/reduce_sum | solution.py:52
  247.6 31.4 %all-to-all-done.1 = bf16[8,128,2048]{2,1,0:T(8,128)(2,1)} async-done(((bf16[8,128,2048]{2,1,0:T(8,128)(2,1)}), bf16[8,128,2048]{2,1,0:T(8,128)(2,1)}, u32[]{:S(2)}, u32[]{:S(2)}) %all-to-all-start.1) | async-done | bytes 4194336 | tf_op jit(solution)/shard_map/all_to_all | solution.py:51
  279.0 3.8 %reduce_sum.25 = bf16[128,2048]{1,0:T(8,128)(2,1)} reduce(bf16[8,128,2048]{2,1,0:T(8,128)(2,1)} %all-to-all-done.1, bf16[]{:T(256)} %constant.8.clone.1), dimensions={0}, to_apply=%region_1.2 | reduce | flops 1835008 | bytes 4718594 | tf_op jit(solution)/shard_map/reduce_sum | solution.py:52
  282.8 1.5 multiply_add_fusion
  284.3 9.4 %reduce-scatter.7.cloned.1.call-done = bf16[64,512]{1,0:T(8,128)(2,1)} async-done(((bf16[256,512]{1,0:T(8,128)(2,1)}), bf16[64,512]{1,0:T(8,128)(2,1)}) %reduce-scatter.7.cloned.1.call-update) | async-done | bytes 65552 | tf_op jit(solution)/shard_map/reduce_scatter | solution.py:58
  293.7 1.5 multiply_add_fusion.1
  (26 shorter events, 0.3 us)
Async XLA Ops:
  7.2 4.1 %copy-start = (bf16[128,2048]{1,0:T(8,128)(2,1)S(1)}, bf16[128,2048]{1,0:T(8,128)(2,1)}, u32[]{:S(2)}) copy-start(bf16[128,2048]{1,0:T(8,128)(2,1)} %param.7) | copy-start | bytes 1572868
  7.2 88.6 %all-gather.3.cloned.1.call-start = ((), (), s32[]{:S(2)}) async-start(), calls=%async_computation.6 | async-start | bytes 4325376 | tf_op jit(solution)/shard_map/all_gather | solution.py:41
  8.8 137.1 %all-gather.5.cloned.1.call-start = ((), (), s32[]{:S(2)}) async-start(), calls=%async_computation.7 | async-start | bytes 9437184 | tf_op jit(solution)/shard_map/all_gather | solution.py:41
  11.2 219.5 %reduce-scatter.9.cloned.1.call-start = ((), (), s32[]{:S(2)}) async-start(), calls=%async_computation.10 | async-start | bytes 2359296 | tf_op jit(solution)/shard_map/reduce_scatter | solution.py:58
  11.3 2.0 collective-permute-start
  13.4 25.8 %collective-permute-start.1 = (bf16[2,128,2048]{2,1,0:T(8,128)(2,1)S(1)}, bf16[2,128,2048]{2,1,0:T(8,128)(2,1)}, u32[]{:S(2)}, u32[]{:S(2)}) collective-permute-start(bf16[2,128,2048]{2,1,0:T(8,128)(2,1)S(1)} %pad_maximum_fusion.2), channel_id=1, source_target_pairs={{0,2},{1,3},{2,0},{3,1},{4,6},{5,7},{6,4},{7,5},{8,10},{9,11},{10,... | collective-permute-start | bytes 3145736 | tf_op jit(solution)/shard_map/ppermute | solution.py:22
  42.1 114.2 %collective-permute-start.2 = (bf16[4,128,2048]{2,1,0:T(8,128)(2,1)}, bf16[4,128,2048]{2,1,0:T(8,128)(2,1)}, u32[]{:S(2)}, u32[]{:S(2)}) collective-permute-start(bf16[4,128,2048]{2,1,0:T(8,128)(2,1)} %pad_maximum_fusion.1), channel_id=1, source_target_pairs={{0,4},{1,5},{2,6},{3,7},{4,0},{5,1},{6,2},{7,3},{8,12},{9,13},{10,... | collective-permute-start | bytes 6291464 | tf_op jit(solution)/shard_map/ppermute | solution.py:22
  145.9 6.7 %copy-start.3 = (bf16[1024,4096]{1,0:T(8,128)(2,1)S(1)}, bf16[1024,4096]{1,0:T(8,128)(2,1)}, u32[]{:S(2)}) copy-start(bf16[1024,4096]{1,0:T(8,128)(2,1)} %all-gather.5.cloned.1.call-done) | copy-start | bytes 25165828
  151.2 1.4 copy-start.4
  170.5 6.0 %copy-start.5 = (f32[1024,512]{1,0:T(8,128)S(1)}, f32[1024,512]{1,0:T(8,128)}, u32[]{:S(2)}) copy-start(f32[1024,512]{1,0:T(8,128)} %copy-done.4) | copy-start | bytes 6291460
  170.5 54.3 %all-to-all-start = ((bf16[8,128,2048]{2,1,0:T(8,128)(2,1)}), bf16[8,128,2048]{2,1,0:T(8,128)(2,1)}, u32[]{:S(2)}, u32[]{:S(2)}) async-start(bf16[8,128,2048]{2,1,0:T(8,128)(2,1)} %bitcast.10), calls=%async_computation | async-start | bytes 8388608 | tf_op jit(solution)/shard_map/all_to_all | solution.py:51
  176.4 67.2 %reduce-scatter.5.cloned.1.call-start = ((), (), s32[]{:S(2)}) async-start(), calls=%async_computation.8 | async-start | bytes 2359296 | tf_op jit(solution)/shard_map/reduce_scatter | solution.py:58
  224.8 54.2 %all-to-all-start.1 = ((bf16[8,128,2048]{2,1,0:T(8,128)(2,1)}), bf16[8,128,2048]{2,1,0:T(8,128)(2,1)}, u32[]{:S(2)}, u32[]{:S(2)}) async-start(bf16[8,128,2048]{2,1,0:T(8,128)(2,1)} %bitcast.9), calls=%async_computation.1 | async-start | bytes 8388608 | tf_op jit(solution)/shard_map/all_to_all | solution.py:51
  230.6 52.2 %reduce-scatter.11.cloned.1.call-start = ((), (), s32[]{:S(2)}) async-start(), calls=%async_computation.11 | async-start | bytes 327680 | tf_op jit(solution)/shard_map/reduce_scatter | solution.py:58
  231.2 62.5 %reduce-scatter.7.cloned.1.call-start = ((), (), s32[]{:S(2)}) async-start(), calls=%async_computation.9 | async-start | bytes 327680 | tf_op jit(solution)/shard_map/reduce_scatter | solution.py:58
  247.6 35.3 %copy-start.1 = (f32[64,512]{1,0:T(8,128)S(1)}, f32[64,512]{1,0:T(8,128)}, u32[]{:S(2)}) copy-start(f32[64,512]{1,0:T(8,128)} %param.13) | copy-start | bytes 393220
  247.6 46.2 %copy-start.2 = (f32[64,512]{1,0:T(8,128)S(1)}, f32[64,512]{1,0:T(8,128)}, u32[]{:S(2)}) copy-start(f32[64,512]{1,0:T(8,128)} %param.12) | copy-start | bytes 393220
Sparse Core Ops, SparseCore 0:
  11.1 84.6 all-gather.2
  97.6 48.1 all-gather.4
  156.4 43.7 reduce-scatter.8
  202.6 41.0 reduce-scatter.4
  246.0 22.0 reduce-scatter.10
  270.5 23.1 reduce-scatter.6
